TPU v7x, 32 devices: a whole 2x2x4 slice. The times are simulated.
32 devices in a mesh: grp: 2 (over y), sp: 4 (over z), tp: 4 (over x, core).
Axes of the slice: x: 2, y: 2, z: 4, core: 2. Of those that a mesh axis runs over, the one named last changes fastest.
Arguments:
- tokens: bfloat16 [2, 2048, 2048], P('grp', ('sp', 'tp')), parts along dimension 0, may hold values from -6 to 6
- norm_gain: bfloat16 [2048], replicated, may hold values from 0.099609375 to 1.8984375
- w_query: bfloat16 [2048, 1024], P('sp'), may hold values from -0.125 to 0.125
- w_forget: bfloat16 [2048, 1024], P('sp'), may hold values from -0.125 to 0.125
- w_input: bfloat16 [2048, 1024], P('sp'), may hold values from -0.125 to 0.125
- floor_gap: float32 [1024], replicated, may hold values from 0.000146484375 to 0.12
- extra_decay: float32 [2, 2048, 16], P('grp', ('sp', 'tp')), parts along dimension 0, may hold values from -1.4 to 0, as said below
- init_state: float32 [2, 16, 64, 64], P('grp'), parts along dimension 0, may hold values from -0.078125 to 0.078125
- head_norm_gain: bfloat16 [1024], replicated, may hold values from 0.099609375 to 1.8984375
- w_output: bfloat16 [1024, 2048], P(None, 'sp'), may hold values from -0.1875 to 0.1875
Outputs:
- mixed: bfloat16 [2, 2048, 2048], P('grp', ('sp', 'tp')), parts along dimension 0
- final_state: float32 [2, 65536], P('grp', ('sp', 'tp')), parts along dimension 0
There are 2 independent parts, one for each index of `grp`. A program takes and returns all parts, laid end to end along the dimension named above; an argument that names none is the same for every part. Nothing has to cross between parts.
Inputs may be any that keep to these rules, and one draw needn't show every extreme that they name: `extra_decay`: no entry is positive.
All inputs are finite; a program needn't handle non-finite values.
Results may differ from a plain program's by a relative error of at most 0.014.
Values may be sent and summed in bfloat16 or wider, within the bound.
A program may use at most 128 MiB of HBM per device.

v0:
```python
import jax
import jax.numpy as jnp
from jax import lax
from jax.sharding import PartitionSpec as P

HEADS = 16
HEAD = 64
BLOCK = 64


EPSILON = 1e-05


def carried_in(value, axis, combine, identity):
    peers, mine = (lax.axis_size(axis), lax.axis_index(axis))
    everything = jax.tree.map(
        lambda part, kind: lax.all_gather(part.astype(kind), axis),
        value,
        (jnp.bfloat16, jnp.bfloat16),
    )
    start = jax.tree.map(
        lambda part, zero: jnp.broadcast_to(jnp.asarray(zero, part.dtype), part.shape),
        value,
        identity,
    )

    def step(k, before):
        reached = k < mine
        new = combine(
            before, jax.tree.map(lambda part, own: part[k].astype(own.dtype), everything, value)
        )
        return jax.tree.map(lambda a, b: jnp.where(reached, a, b), new, before)

    return lax.fori_loop(0, peers, step, start)


def broadcast(block, axis, source):
    block = jnp.where(lax.axis_index(axis) == source, block, jnp.zeros_like(block))
    return lax.psum(block, axis)


def layer_normed(tokens, norm_gain):
    values = tokens.astype(jnp.float32)
    center = values - jnp.mean(values, axis=-1, keepdims=True)
    spread = jnp.mean(center * center, axis=-1, keepdims=True)
    return (center * lax.rsqrt(spread + EPSILON) * norm_gain.astype(jnp.float32)).astype(
        jnp.bfloat16
    )


def gate_terms(query_sum, forget_sum, input_sum, floor_gap, extra_decay):
    query_raw = query_sum.astype(jnp.bfloat16)
    forget_raw = forget_sum.astype(jnp.bfloat16)
    input_raw = input_sum.astype(jnp.bfloat16)
    forget_pre = forget_raw.astype(jnp.float32)
    split_shape = forget_pre.shape[:-1] + (HEADS, HEAD)
    log_keep = jnp.logaddexp(
        jnp.log1p(-floor_gap), jnp.log(floor_gap) + jax.nn.log_sigmoid(forget_pre)
    )
    log_keep = log_keep.reshape(split_shape) + extra_decay[..., None]
    key_gate = (floor_gap * jax.nn.sigmoid(-forget_pre)).reshape(split_shape)
    query = jax.nn.silu(query_raw.astype(jnp.float32)).reshape(split_shape)
    values = input_raw.astype(jnp.float32).reshape(split_shape)
    return (query, key_gate, values, log_keep)


def block_pass(query, key_gate, values, log_keep):
    highest = lax.Precision.HIGHEST
    cumul = jnp.cumsum(log_keep, axis=2)
    q_decayed = query * jnp.exp(cumul)
    key_decayed = key_gate * jnp.exp(-cumul)
    causal = lax.broadcasted_iota(jnp.int32, (BLOCK, BLOCK), 0) >= lax.broadcasted_iota(
        jnp.int32, (BLOCK, BLOCK), 1
    )
    scores = jnp.einsum("snthd,snuhd->snhtu", q_decayed, key_decayed, precision=highest)
    scores = jnp.where(causal, scores, 0.0)
    within = jnp.einsum("snhtu,snuhe->snthe", scores, values, precision=highest)
    totals = cumul[:, :, -1]
    k_tail = key_gate * jnp.exp(totals[:, :, None] - cumul)
    block_state = jnp.einsum("snthd,snthe->snhde", k_tail, values, precision=highest)
    return (q_decayed, within, totals, block_state)


def linked_advance(earlier, later):
    return (earlier[0] + later[0], jnp.exp(later[0])[..., None] * earlier[1] + later[1])


def read_out(q_global, leading_logarithm, prefix_state, init_part):
    carried = jnp.exp(leading_logarithm)[..., None] * init_part + prefix_state
    added = jnp.einsum("snthd,shde->snthe", q_global, carried, precision=lax.Precision.HIGHEST)
    return (carried, added)


def body(
    tokens,
    norm_gain,
    w_query,
    w_forget,
    w_input,
    floor_gap,
    extra_decay,
    init_state,
    head_norm_gain,
    w_output,
):
    normed = layer_normed(tokens, norm_gain)
    seqs, span = (tokens.shape[0], tokens.shape[1])

    def add_rows(piece):
        return jnp.dot(normed, piece, preferred_element_type=jnp.float32)

    query_sum = add_rows(lax.all_gather(w_query, "sp", axis=0, tiled=True))
    forget_sum = add_rows(lax.all_gather(w_forget, "sp", axis=0, tiled=True))
    input_sum = add_rows(lax.all_gather(w_input, "sp", axis=0, tiled=True))
    query, key_gate, values, log_keep = gate_terms(
        query_sum, forget_sum, input_sum, floor_gap, extra_decay
    )
    blocks = span // BLOCK
    blocked = (seqs, blocks, BLOCK, HEADS, HEAD)
    q_decayed, within, totals, block_state = block_pass(
        query.reshape(blocked),
        key_gate.reshape(blocked),
        values.reshape(blocked),
        log_keep.reshape(blocked),
    )
    running_state = jnp.zeros((seqs, HEADS, HEAD, HEAD), jnp.float32)
    running_log = jnp.zeros((seqs, HEADS, HEAD), jnp.float32)
    entering_list = []
    offset_list = []
    for number in range(blocks):
        entering_list.append(running_state)
        offset_list.append(running_log)
        running_state = (
            jnp.exp(totals[:, number])[..., None] * running_state + block_state[:, number]
        )
        running_log = running_log + totals[:, number]
    entering = jnp.stack(entering_list, axis=1)
    offsets = jnp.stack(offset_list, axis=1)
    local_out = within + jnp.einsum(
        "snthd,snhde->snthe", q_decayed, entering, precision=lax.Precision.HIGHEST
    )
    q_global = q_decayed * jnp.exp(offsets[:, :, None])
    leading_logarithm, prefix_state = carried_in(
        (running_log, running_state),
        ("sp", "tp"),
        linked_advance,
        (jnp.zeros_like(running_log), jnp.zeros_like(running_state)),
    )
    carried, added = read_out(q_global, leading_logarithm, prefix_state, init_state)
    flat_total = HEADS * HEAD * HEAD
    piece_count = flat_total // lax.axis_size(("sp", "tp"))
    piece_start = lax.axis_index(("sp", "tp")) * piece_count
    after_state = (jnp.exp(running_log)[..., None] * carried + running_state).reshape(
        seqs, flat_total
    )
    whole_state = broadcast(
        after_state.astype(jnp.bfloat16), ("sp", "tp"), lax.axis_size(("sp", "tp")) - 1
    ).astype(after_state.dtype)
    final_state = lax.dynamic_slice_in_dim(whole_state, piece_start, piece_count, 1)
    recurrent = (local_out + added).reshape(seqs, span, HEADS, HEAD)
    average_power = jnp.mean(recurrent * recurrent, axis=-1, keepdims=True)
    scaled = (
        recurrent
        * lax.rsqrt(average_power + EPSILON)
        * head_norm_gain.astype(jnp.float32).reshape(HEADS, HEAD)
    )
    gated = scaled.reshape(seqs, span, HEADS * HEAD).astype(jnp.bfloat16)
    mixed = jnp.dot(
        gated,
        lax.all_gather(w_output, "sp", axis=1, tiled=True),
        preferred_element_type=jnp.float32,
    ).astype(jnp.bfloat16)
    return (mixed, final_state)


def solution(mesh):
    placed = (
        P("grp", ("sp", "tp"), None),
        P(),
        P("sp", None),
        P("sp", None),
        P("sp", None),
        P(),
        P("grp", ("sp", "tp"), None),
        P("grp", None, None, None),
        P(),
        P(None, "sp"),
    )
    return jax.shard_map(
        body,
        mesh=mesh,
        in_specs=placed,
        out_specs=(P("grp", ("sp", "tp"), None), P("grp", ("sp", "tp"))),
        check_vma=False,
    )
```

profile of v0, /device:TPU:0, one launch (start us, length us, event | category | flops | bytes accessed | tf_op | source)
XLA Modules:
  0.0 493.7 jit_solution(17431788789680109495)
XLA Ops:
  7.2 0.0 all-gather.10.cloned.1.call-start
  7.2 0.7 all-gather.10.cloned.1.call-update
  7.9 0.0 all-gather.8.cloned.1.call-start
  8.0 0.7 all-gather.8.cloned.1.call-update
  8.7 0.0 all-gather.6.cloned.1.call-start
  8.7 0.7 all-gather.6.cloned.1.call-update
  9.4 0.0 all-gather.12.cloned.1.call-start
  9.5 0.7 convert_element_type.119
  10.1 0.8 copy.63
  10.9 1.2 convert_reduce_fusion
  12.1 1.3 fusion.9
  13.5 79.6 %all-gather.10.cloned.1.call-done = bf16[2048,1024]{1,0:T(8,128)(2,1)} async-done(((bf16[512,1024]{1,0:T(8,128)(2,1)}), bf16[2048,1024]{1,0:T(8,128)(2,1)}) %all-gather.10.cloned.1.call-update) | async-done | bytes 4194320 | tf_op jit(solution)/shard_map/all_gather | solution.py:113
  93.1 3.7 add_select_fusion.1
  96.8 0.3 reshape.392
  97.1 1.3 reshape_reshape.8
  98.4 75.5 %all-gather.8.cloned.1.call-done = bf16[2048,1024]{1,0:T(8,128)(2,1)} async-done(((bf16[512,1024]{1,0:T(8,128)(2,1)}), bf16[2048,1024]{1,0:T(8,128)(2,1)}) %all-gather.8.cloned.1.call-update) | async-done | bytes 4194320 | tf_op jit(solution)/shard_map/all_gather | solution.py:112
  173.9 3.0 divide_multiply_fusion.1
  177.0 1.3 reshape_reshape.7
  178.2 0.4 fusion.22
  178.7 76.1 %all-gather.6.cloned.1.call-done = bf16[2048,1024]{1,0:T(8,128)(2,1)} async-done(((bf16[512,1024]{1,0:T(8,128)(2,1)}), bf16[2048,1024]{1,0:T(8,128)(2,1)}) %all-gather.6.cloned.1.call-update) | async-done | bytes 4194320 | tf_op jit(solution)/shard_map/all_gather | solution.py:114
  254.8 2.9 convolution_convert_fusion.3
  257.8 0.3 reshape.391
  258.1 3.3 fusion.18
  261.5 1.2 convolution_bitcast_fusion.1
  262.7 1.2 add_convert_fusion
  263.9 0.0 all-gather.12.cloned.1.call-update
  263.9 0.0 all-gather.14.cloned.1.call-start
  263.9 0.5 all-gather.14.cloned.1.call-update
  264.5 0.0 all-reduce.4.cloned.1.call-start
  264.6 0.0 copy-start.1
  264.6 19.4 %all_gather.23 = bf16[16,1,16,64]{3,2,1,0:T(8,128)(2,1)S(1)} all-gather(bf16[1,1,16,64]{3,2,1,0:T(8,128)(2,1)S(1)} %get-tuple-element.162), channel_id=1, replica_groups=mesh['grp'=2,'sp'=4,'tp'=4] {'sp','tp'}, dimensions={0}, use_global_device_ids=true | all-gather | bytes 34816 | tf_op jit(solution)/shard_map/all_gather | solution.py:17
  284.0 3.6 convolution_select_fusion
  287.6 1.0 fusion.34
  288.6 3.1 fusion.3
  291.7 21.5 %all-gather.12.cloned.1.call-done = bf16[16,1,16,64,64]{4,3,2,1,0:T(8,128)(2,1)} async-done(((bf16[1,1,16,64,64]{4,3,2,1,0:T(8,128)(2,1)}), bf16[16,1,16,64,64]{4,3,2,1,0:T(8,128)(2,1)}) %all-gather.12.cloned.1.call-update) | async-done | bytes 2097168 | tf_op jit(solution)/shard_map/all_gather | solution.py:17
  313.2 22.0 %while.16 = (s32[]{:T(128)}, f32[1,16,64]{2,1,0:T(8,128)S(1)}, f32[1,16,64,64]{3,2,1,0:T(8,128)S(1)}, s32[]{:T(128)}, bf16[16,1,16,64]{3,2,1,0:T(8,128)(2,1)S(1)...) while((s32[]{:T(128)}, f32[1,16,64]{2,1,0:T(8,128)S(1)}, ...), condition=%wide.region_4.5_spmd.clone, body=%wide.region_3.4_spmd.clone.sunk | while | flops 332804 | bytes 675959 | solution.py:34
  313.3 1.4 fusion.53
  314.7 1.3 fusion.53
  316.1 1.3 fusion.53
  317.4 1.3 fusion.53
  318.8 1.3 fusion.53
  320.2 1.3 fusion.53
  321.6 1.3 fusion.53
  322.9 1.3 fusion.53
  324.3 1.3 fusion.53
  325.7 1.3 fusion.53
  327.1 1.3 fusion.53
  328.4 1.3 fusion.53
  329.8 1.3 fusion.53
  331.1 1.3 fusion.53
  332.5 1.3 fusion.53
  333.9 1.3 fusion.53
  335.2 0.7 fusion.37
  336.0 0.9 select_n.80
  336.8 5.6 %multiply_reduce_fusion = (f32[2,64,16]{1,2,0:T(8,128)S(1)}, f32[1,2,64,16,64]{2,4,3,1,0:T(8,128)}) fusion(f32[1,2,64,16,64]{2,4,3,1,0:T(8,128)} %fusion.3, f32[2,64,16,64]{3,2,1,0:T(8,128)S(1)} %copy-done, f32[1,16,64,64]{3,2,1,0:T(8,128)S(1)} %get-tuple-element.113, f32[1,16,64,64]{3,2,1,0:T(8,128)S(1)} %copy-done.3, ...), kind=kOutput, calls=%fused_computation.39 | convolution fusion | flops 101185536 | bytes 2109440 | tf_op jit(solution)/shard_map/snthd,shde->snthe/dot_general | solution.py:90
  342.4 1.7 copy.56
  344.2 0.3 reshape.395
  344.5 0.1 rsqrt.21
  344.6 0.2 copy.58
  344.8 0.0 all-reduce.4.cloned.1.call-update
  344.9 49.1 %all-gather.14.cloned.1.call-done = bf16[1024,2048]{1,0:T(8,128)(2,1)} async-done(((bf16[1024,512]{1,0:T(8,128)(2,1)}), bf16[1024,2048]{1,0:T(8,128)(2,1)}) %all-gather.14.cloned.1.call-update) | async-done | bytes 4194320 | tf_op jit(solution)/shard_map/all_gather | solution.py:170
  394.0 3.7 fusion.2
  397.7 87.8 %all-reduce.4.cloned.1.call-done = bf16[1,65536]{1,0:T(2,128)(2,1)} async-done(((bf16[1,65536]{1,0:T(2,128)(2,1)}), bf16[1,65536]{1,0:T(2,128)(2,1)}) %all-reduce.4.cloned.1.call-update) | async-done | bytes 131088 | tf_op jit(solution)/shard_map/psum | solution.py:39
  485.5 1.3 dynamic-slice_convert_fusion
  (57 shorter events, 0.5 us)
Async XLA Ops:
  7.2 86.0 %copy-start.2 = (bf16[1,128,2048]{2,1,0:T(8,128)(2,1)S(1)}, bf16[1,128,2048]{2,1,0:T(8,128)(2,1)}, u32[]{:S(2)}) copy-start(bf16[1,128,2048]{2,1,0:T(8,128)(2,1)} %param.12) | copy-start | bytes 1572868
  7.2 6.3 %copy-start.4 = (f32[1024]{0:T(1024)S(1)}, f32[1024]{0:T(1024)}, u32[]{:S(2)}) copy-start(f32[1024]{0:T(1024)} %param.17) | copy-start | bytes 12292
  7.2 85.9 %all-gather.10.cloned.1.call-start = ((), (), s32[]{:S(2)}) async-start(), calls=%async_computation.2 | async-start | bytes 5242880 | tf_op jit(solution)/shard_map/all_gather | solution.py:113
  7.9 166.0 %all-gather.8.cloned.1.call-start = ((), (), s32[]{:S(2)}) async-start(), calls=%async_computation.1 | async-start | bytes 5242880 | tf_op jit(solution)/shard_map/all_gather | solution.py:112
  8.7 246.1 %all-gather.6.cloned.1.call-start = ((), (), s32[]{:S(2)}) async-start(), calls=%async_computation | async-start | bytes 5242880 | tf_op jit(solution)/shard_map/all_gather | solution.py:114
  9.4 303.8 %all-gather.12.cloned.1.call-start = ((), (), s32[]{:S(2)}) async-start(), calls=%async_computation.3 | async-start | bytes 4456448 | tf_op jit(solution)/shard_map/all_gather | solution.py:17
  261.5 3.1 copy-start.5
  263.9 130.1 %all-gather.14.cloned.1.call-start = ((), (), s32[]{:S(2)}) async-start(), calls=%async_computation.4 | async-start | bytes 5242880 | tf_op jit(solution)/shard_map/all_gather | solution.py:170
  264.5 221.0 %all-reduce.4.cloned.1.call-start = ((), (), s32[]{:S(2)}) async-start(), calls=%async_computation.5 | async-start | bytes 524288 | tf_op jit(solution)/shard_map/psum | solution.py:39
  264.6 24.0 %copy-start.1 = (f32[1,1,16,64,64]{4,3,2,1,0:T(8,128)S(1)}, f32[1,1,16,64,64]{4,3,2,1,0:T(8,128)}, u32[]{:S(2)}) copy-start(f32[1,1,16,64,64]{4,3,2,1,0:T(8,128)} %get-tuple-element.148) | copy-start | bytes 786436
  291.7 43.5 %copy-start.3 = (f32[1,16,64,64]{3,2,1,0:T(8,128)S(1)}, f32[1,16,64,64]{3,2,1,0:T(8,128)}, u32[]{:S(2)}) copy-start(f32[1,16,64,64]{3,2,1,0:T(8,128)} %param.19) | copy-start | bytes 786436
  313.2 23.6 %copy-start = (f32[2,64,16,64]{3,2,1,0:T(8,128)S(1)}, f32[2,64,16,64]{3,2,1,0:T(8,128)}, u32[]{:S(2)}) copy-start(f32[2,64,16,64]{3,2,1,0:T(8,128)} %get-tuple-element.153) | copy-start | bytes 1572868
Sparse Core Ops, SparseCore 0:
  9.6 83.5 all-gather.9
  94.7 79.2 all-gather.7
  175.5 79.2 all-gather.5
  264.0 49.1 all-gather.11
  314.7 79.2 all-gather.13
  397.2 88.2 all-reduce.3
where the time goes:
time: 495 us; the launch traced here: 494 us
  waiting for transfers between devices  392 us (79%)
  other arithmetic  31.6 us (6%)
  matrix products  27.9 us (6%)
  blocking collectives  19.4 us (4%)
  between operations  14.3 us (3%)
  local copies, waits for them, and re-layouts  7.27 us (1%)
    psum x1, waiting for transfers between devices, broadcast(): return lax.psum(block, axis)  87.8 us
    all_gather x1, waiting for transfers between devices, body(): forget_sum = add_rows(lax.all_gather(w_forget, 'sp', axis=0, tiled=True))  79.6 us
    all_gather x1, waiting for transfers between devices, body(): input_sum = add_rows(lax.all_gather(w_input, 'sp', axis=0, tiled=True))  76.1 us
    all_gather x1, waiting for transfers between devices, body(): query_sum = add_rows(lax.all_gather(w_query, 'sp', axis=0, tiled=True))  75.5 us
    all_gather x1, waiting for transfers between devices, body(): lax.all_gather(w_output, 'sp', axis=1, tiled=True)  49.1 us
    all_gather x1, waiting for transfers between devices, carried_in(): lax.all_gather(part.astype(kind), axis)  21.5 us
    select_n x32, other arithmetic, step(): return jax.tree.map(lambda a, b: jnp.where(reached, a, b), new, before)  21.1 us
    all_gather x1, blocking collectives, carried_in(): lax.all_gather(part.astype(kind), axis)  19.4 us
  transfers between devices with their start and end apart: 6, of which 6 were waited for; matrix products, arithmetic and copies ran while one was open for 11% of the time, Pallas kernels for 0%

commit v1 on v0

v1 whole, which is shorter than its diff:
```python
import functools

import jax
import jax.numpy as jnp
from jax import lax
from jax.experimental import pallas as pl
from jax.experimental.pallas import tpu as pltpu
from jax.sharding import PartitionSpec as P

HEAD = 64
BLOCK = 64
CORES = 2
LANES = 128
EPSILON = 1e-05
F32, BF16 = jnp.float32, jnp.bfloat16
HIGHEST = lax.Precision.HIGHEST


def contract(a, b, da, db, precision=None):
    return lax.dot_general(
        a, b, (((da,), (db,)), ((), ())), precision=precision, preferred_element_type=F32
    )


def iota(shape, dim):
    return lax.broadcasted_iota(jnp.int32, shape, dim)


def same_group(rows, cols, size):
    return iota((rows, cols), 0) // size == iota((rows, cols), 1) // size


def swap_halves(a):
    return jnp.concatenate([a[:, HEAD:], a[:, :HEAD]], axis=1)


def kernel(
    sizes,
    tokens, norm_gain, w_query, w_forget, w_input, gap, extra, init, head_gain, w_output,
    mixed, final,
    tok, ext, nrm, wbuf, wout, start, qd, kd, val, etot, bstate, within, gated, carried,
    st_send, st_recv, dk_send, dk_recv, fin, fin_recv, a_send, a_recv, b_send, b_recv,
    loc, tok_s, tok_r, ext_s, ext_r, z_s, z_r, y_s, y_r, oz_s, oz_r, oy_s, oy_r,
    st_s, st_r, dk_s, dk_r, fin_s, fin_r, as_, ar_, bs_, br_,
):
    ng, ns, nt, span, D, C, O, chunks = sizes
    g, s, t = lax.axis_index("grp"), lax.axis_index("sp"), lax.axis_index("tp")
    R, OC = D // ns, O // ns
    Rh, Ch = R // ng, C // ng
    nx = nt // CORES
    T = nt * span
    nblk, per = T // BLOCK, span // BLOCK
    G = C // LANES
    fold = G % 2 == 0
    weights = (w_query, w_forget, w_input)
    own_cols = pl.ds(pl.multiple_of(t * C, LANES), C)

    def remote(src, dst, ssem, rsem, where):
        return pltpu.make_async_remote_copy(
            src_ref=src, dst_ref=dst, send_sem=ssem, recv_sem=rsem,
            device_id=where, device_id_type=pl.DeviceIdType.MESH,
        )

    def piece(k, a, who):
        return wbuf.at[pl.ds(pl.multiple_of(k * R + who * Rh, 16), Rh), pl.ds(a * C, C)]

    def z_copy(k, a, way, src):
        to = s + 1 if way == 0 else s - 1
        return remote(src, piece(k, a, g), z_s.at[way, k, a], z_r.at[k, a], {"sp": to})

    def y_copy(k, a, dy, who):
        return remote(
            piece(k, a, who), piece(k, a, who), y_s.at[dy - 1, k, a], y_r.at[dy - 1, k, a],
            {"grp": lax.rem(g + dy, ng)},
        )

    def o_piece(k, who):
        return wout.at[
            pl.ds(pl.multiple_of(who * Ch, 16), Ch), pl.ds(pl.multiple_of(k * OC, LANES), OC)
        ]

    def oz_copy(k, dz):
        src = w_output.at[pl.ds(pl.multiple_of(t * C + g * Ch, 16), Ch), :]
        return remote(
            src, o_piece(k, g), oz_s.at[dz], oz_r.at[dz], {"sp": lax.rem(s + dz, ns)}
        )

    def oy_copy(k, dz, dy, who):
        return remote(
            o_piece(k, who), o_piece(k, who), oy_s.at[dy - 1, dz], oy_r.at[dy - 1, dz],
            {"grp": lax.rem(g + dy, ng)},
        )

    def tok_copy(dt, slot):
        return remote(
            tokens, tok.at[slot], tok_s.at[dt], tok_r.at[dt], {"tp": lax.rem(t + dt, nt)}
        )

    def ext_copy(dt, slot):
        return remote(
            extra, ext.at[slot], ext_s.at[dt], ext_r.at[dt], {"tp": lax.rem(t + dt, nt)}
        )

    for a in range(3):
        own = weights[a].at[pl.ds(pl.multiple_of(g * Rh, 16), Rh), own_cols]

        @pl.when(s < ns - 1)
        def _():
            z_copy(s, a, 0, own).start()

        @pl.when(s > 0)
        def _():
            z_copy(s, a, 1, own).start()

    for dt in range(1, nt):
        tok_copy(dt, t).start()
        ext_copy(dt, t).start()
    locals_ = [
        pltpu.make_async_copy(tokens, tok.at[t], loc.at[0]),
        pltpu.make_async_copy(extra, ext.at[t], loc.at[1]),
        pltpu.make_async_copy(
            init.at[pl.ds(pl.multiple_of(t * C, LANES), C), :], start, loc.at[2]
        ),
        pltpu.make_async_copy(
            w_output.at[pl.ds(pl.multiple_of(t * C, LANES), C), :],
            wout.at[:, pl.ds(pl.multiple_of(s * OC, LANES), OC)],
            loc.at[3],
        ),
    ] + [
        pltpu.make_async_copy(
            weights[a].at[:, own_cols],
            wbuf.at[pl.ds(pl.multiple_of(s * R, 16), R), pl.ds(a * C, C)],
            loc.at[4 + a],
        )
        for a in range(3)
    ]
    for copy in locals_:
        copy.start()

    def normalize(slot):
        rows = 32

        def step(i, _):
            x = tok[slot, pl.ds(pl.multiple_of(i * rows, rows), rows), :].astype(F32)
            center = x - jnp.mean(x, axis=-1, keepdims=True)
            spread = jnp.mean(center * center, axis=-1, keepdims=True)
            nrm[pl.ds(pl.multiple_of(slot * span + i * rows, rows), rows), :] = (
                center * lax.rsqrt(spread + EPSILON) * norm_gain[...]
            ).astype(BF16)
            return 0

        lax.fori_loop(0, span // rows, step, 0)

    locals_[0].wait()
    normalize(t)

    for d in range(max(ns - 1, nt - 1)):
        if d < ns - 1:
            for a in range(3):
                for way in range(2):
                    k = s - 1 - d if way == 0 else s + 1 + d
                    valid = k >= 0 if way == 0 else k < ns
                    more = s < ns - 1 if way == 0 else s > 0

                    @pl.when(valid)
                    def _():
                        z_copy(k, a, way, piece(k, a, g)).wait_recv()

                        @pl.when(more)
                        def _():
                            z_copy(k, a, way, piece(k, a, g)).start()

                        for dy in range(1, ng):
                            y_copy(k, a, dy, g).start()
            if d == ns - 2:
                for dz in range(1, ns):
                    oz_copy(s, dz).start()
        if d < nt - 1:
            slot = lax.rem(t + nt - 1 - d, nt)
            tok_copy(d + 1, slot).wait_recv()
            normalize(slot)
            ext_copy(d + 1, slot).wait_recv()

    for copy in locals_[1:]:
        copy.wait()

    diag = same_group(C, C, HEAD)
    spread_eye = (lax.rem(iota((C, HEAD), 0), HEAD) == iota((C, HEAD), 1)).astype(F32)
    flipped = contract(spread_eye, start[...], 1, 1, HIGHEST)

    def y_wait(k, a):
        for dy in range(1, ng):
            y_copy(k, a, dy, lax.rem(g + ng - dy, ng)).wait_recv()

    for dz in range(1, ns):
        for a in range(3):
            y_wait(lax.rem(s + dz, ns), a)

    floor = gap[:, own_cols]
    heads = (
        iota((LANES, C), 0) == iota((LANES, C), 1) // HEAD + t * (C // HEAD)
    ).astype(F32)
    tri = (
        (iota((span, span), 0) >= iota((span, span), 1)) & same_group(span, span, BLOCK)
    ).astype(F32)
    carried[...] = jnp.zeros_like(carried)
    dk_send[...] = jnp.ones_like(dk_send)

    def project(m, _):
        rows = pl.ds(pl.multiple_of(m * span, span), span)
        x = nrm[rows, :]
        raw = [
            jnp.dot(x, wbuf[:, a * C:(a + 1) * C], preferred_element_type=F32).astype(BF16)
            for a in range(3)
        ]
        query = raw[0].astype(F32)
        query = query / (1.0 + jnp.exp(-query))
        key = floor / (1.0 + jnp.exp(raw[1].astype(F32)))
        log_keep = jnp.log1p(-key) + jnp.dot(
            ext[m], heads, precision=HIGHEST, preferred_element_type=F32
        )
        cumul = jnp.dot(tri, log_keep, precision=HIGHEST, preferred_element_type=F32)
        qd[rows, :] = (query * jnp.exp(cumul)).astype(BF16)
        kd[rows, :] = (key * jnp.exp(-cumul)).astype(BF16)
        val[rows, :] = raw[2]
        for b in range(per):
            part = slice(b * BLOCK, (b + 1) * BLOCK)
            total = cumul[(b + 1) * BLOCK - 1:(b + 1) * BLOCK, :]
            tail = (key[part] * jnp.exp(total - cumul[part])).astype(BF16)
            state = jnp.where(diag, contract(raw[2][part], tail, 0, 0), 0.0)
            decay = jnp.exp(total)
            n = m * per + b
            bstate[n] = state
            etot[n] = jnp.broadcast_to(decay, etot.shape[1:])
            carried[...] = carried[...] * decay + state
            dk_send[...] = dk_send[...] * decay
        return 0

    lax.fori_loop(0, nt, project, 0)

    tiles = [slice(i * LANES, (i + 1) * LANES) for i in range(G)]
    if fold:
        for i in range(G // 2):
            st_send[tiles[i], :] = (
                carried[tiles[2 * i], tiles[2 * i]]
                + swap_halves(carried[tiles[2 * i + 1], tiles[2 * i + 1]])
            ).astype(BF16)
    else:
        for i in range(G):
            st_send[tiles[i], :] = carried[tiles[i], tiles[i]].astype(BF16)

    def st_copy(dz, slot):
        return remote(st_send, st_recv.at[slot], st_s.at[dz], st_r.at[slot], {"sp": s + dz})

    def dk_copy(dz, slot):
        return remote(dk_send, dk_recv.at[slot], dk_s.at[dz], dk_r.at[slot], {"sp": s + dz})

    for dz in range(1, ns):
        @pl.when(s + dz < ns)
        def _():
            st_copy(dz, s).start()
            dk_copy(dz, s).start()

    for dz in range(1, ns):
        k = lax.rem(s + ns - dz, ns)
        oz_copy(k, dz).wait_recv()
        for dy in range(1, ng):
            oy_copy(k, dz, dy, g).start()

    copies = C // HEAD
    wide = copies * BLOCK
    causal = iota((BLOCK, wide), 0) >= lax.rem(iota((BLOCK, wide), 1), BLOCK)

    def inside(n, _):
        rows = pl.ds(pl.multiple_of(n * BLOCK, BLOCK), BLOCK)
        keys = jnp.where(diag, jnp.concatenate([kd[rows, :]] * copies, axis=0), 0.0)
        vals = jnp.where(diag, jnp.concatenate([val[rows, :]] * copies, axis=0), 0.0)
        scores = contract(qd[rows, :], keys.astype(BF16), 1, 1)
        scores = jnp.where(causal, scores, 0.0).astype(BF16)
        within[rows, :] = jnp.dot(scores, vals.astype(BF16), preferred_element_type=F32)
        return 0

    lax.fori_loop(0, nblk, inside, 0)

    carried[...] = jnp.where(diag, flipped, 0.0)
    near = same_group(LANES, LANES, HEAD)
    for k in range(ns - 1):
        @pl.when(k < s)
        def _():
            st_copy(1, k).wait_recv()
            dk_copy(1, k).wait_recv()
            decay = dk_recv[k][0:1, :]
            for i in range(G):
                packed = st_recv[k, tiles[i // 2] if fold else tiles[i], :].astype(F32)
                if fold and i % 2 == 1:
                    packed = swap_halves(packed)
                carried[tiles[i], tiles[i]] = carried[tiles[i], tiles[i]] * decay[
                    :, tiles[i]
                ] + jnp.where(near, packed, 0.0)

    ones = diag.astype(BF16)
    gain = head_gain[:, own_cols]

    def read(n, _):
        rows = pl.ds(pl.multiple_of(n * BLOCK, BLOCK), BLOCK)
        state = carried[...]
        out = within[rows, :] + contract(qd[rows, :], state.astype(BF16), 1, 1)
        power = jnp.dot((out * out).astype(BF16), ones, preferred_element_type=F32)
        gated[rows, :] = (
            out * lax.rsqrt(power * (1.0 / HEAD) + EPSILON) * gain
        ).astype(BF16)
        carried[...] = state * etot[n][0:1, :] + bstate[n]
        return 0

    lax.fori_loop(0, nblk, read, 0)

    rows_each = final.shape[0]
    here = s * nt + t

    def fin_copy(i, where):
        return remote(
            fin.at[pl.ds(i * rows_each, rows_each), :], fin_recv, fin_s.at[i], fin_r.at[0],
            {"sp": lax.div(where, nt), "tp": lax.rem(where, nt)},
        )

    own_piece = (s == ns - 1) & (here // ns == t)

    @pl.when(s == ns - 1)
    def _():
        fin[...] = contract(carried[...], spread_eye, 0, 0, HIGHEST)
        for i in range(ns):
            where = t * ns + i

            @pl.when(where != here)
            def _():
                fin_copy(i, where).start()

            @pl.when(where == here)
            def _():
                final[...] = fin[i * rows_each:(i + 1) * rows_each, :]

    for dz in range(1, ns):
        k = lax.rem(s + ns - dz, ns)
        for dy in range(1, ng):
            oy_copy(k, dz, dy, lax.rem(g + ng - dy, ng)).wait_recv()

    chip, core = lax.div(t, CORES), lax.rem(t, CORES)
    cw = O // chunks

    def product(dx, side, j):
        block = lax.rem(chip + dx, nx) * CORES + side
        x = gated[pl.ds(pl.multiple_of(block * span, span), span), :]
        return jnp.dot(x, wout[:, j * cw:(j + 1) * cw], preferred_element_type=F32)

    def a_copy(dx, j):
        return remote(
            a_send.at[dx, j], a_recv.at[dx, j], as_.at[dx, j], ar_.at[dx, j],
            {"tp": chip * CORES + 1 - core},
        )

    def b_copy(dx, j):
        return remote(
            b_send.at[dx, j], b_recv.at[dx, j], bs_.at[dx, j], br_.at[dx, j],
            {"tp": lax.rem(chip + dx, nx) * CORES + core},
        )

    order = list(range(1, nx)) + [0]
    for dx in order:
        for j in range(chunks):
            a_send[dx, j] = product(dx, 1 - core, j).astype(BF16)
            a_copy(dx, j).start()
        if dx:
            for j in range(chunks):
                mine = product(dx, core, j)
                a_copy(dx, j).wait_recv()
                b_send[dx, j] = (mine + a_recv[dx, j].astype(F32)).astype(BF16)
                b_copy(dx, j).start()
    for j in range(chunks):
        total = product(0, core, j)
        a_copy(0, j).wait_recv()
        total = total + a_recv[0, j].astype(F32)
        for dx in range(1, nx):
            b_copy(dx, j).wait_recv()
            total = total + b_recv[dx, j].astype(F32)
        mixed[:, j * cw:(j + 1) * cw] = total.astype(BF16)

    @pl.when(jnp.logical_not(own_piece))
    def _():
        fin_copy(0, here).wait_recv()
        final[...] = fin_recv[...]

    for a in range(3):
        for way in range(2):
            more = s < ns - 1 if way == 0 else s > 0
            for d in range(ns):
                k = s - d if way == 0 else s + d
                valid = k >= 0 if way == 0 else k < ns

                @pl.when(valid & more)
                def _():
                    z_copy(k, a, way, piece(k, a, g)).wait_send()
        for dz in range(1, ns):
            for dy in range(1, ng):
                y_copy(lax.rem(s + dz, ns), a, dy, g).wait_send()
    for dt in range(1, nt):
        tok_copy(dt, t).wait_send()
        ext_copy(dt, t).wait_send()
    for dz in range(1, ns):
        oz_copy(s, dz).wait_send()
        for dy in range(1, ng):
            oy_copy(lax.rem(s + ns - dz, ns), dz, dy, g).wait_send()

        @pl.when(s + dz < ns)
        def _():
            st_copy(dz, s).wait_send()
            dk_copy(dz, s).wait_send()

    @pl.when(s == ns - 1)
    def _():
        for i in range(ns):
            @pl.when(t * ns + i != here)
            def _():
                fin_copy(i, t * ns + i).wait_send()

    for dx in order:
        for j in range(chunks):
            a_copy(dx, j).wait_send()
            if dx:
                b_copy(dx, j).wait_send()


def body(
    tokens, norm_gain, w_query, w_forget, w_input, floor_gap, extra_decay, init_state,
    head_norm_gain, w_output,
):
    ng, ns, nt = lax.axis_size("grp"), lax.axis_size("sp"), lax.axis_size("tp")
    span, D = tokens.shape[1:]
    width, heads = w_query.shape[1], extra_decay.shape[2]
    C = width // nt
    O = w_output.shape[1] * ns
    chunks = 4
    T, nblk, nx = nt * span, nt * span // BLOCK, nt // CORES
    pack = C // 2 if (C // LANES) % 2 == 0 else C
    rows_each = width // (ns * nt)
    cw = O // chunks
    V, DMA = pltpu.VMEM, pltpu.SemaphoreType.DMA
    any_, vmem = pl.BlockSpec(memory_space=pl.ANY), pl.BlockSpec(memory_space=pltpu.VMEM)
    extra = jnp.pad(extra_decay[0], ((0, 0), (0, LANES - heads)))
    oth = max(ng - 1, 1)
    mixed, final = pl.pallas_call(
        functools.partial(kernel, (ng, ns, nt, span, D, C, O, chunks)),
        out_shape=(
            jax.ShapeDtypeStruct((span, O), BF16),
            jax.ShapeDtypeStruct((rows_each, HEAD), F32),
        ),
        in_specs=[any_, vmem, any_, any_, any_, vmem, any_, any_, vmem, any_],
        out_specs=(vmem, vmem),
        scratch_shapes=[
            V((nt, span, D), BF16), V((nt, span, LANES), F32), V((T, D), BF16),
            V((D, 3 * C), BF16), V((C, O), BF16), V((C, HEAD), F32),
            V((T, C), BF16), V((T, C), BF16), V((T, C), BF16),
            V((nblk, 8, C), F32), V((nblk, C, C), F32), V((T, C), F32), V((T, C), BF16),
            V((C, C), F32),
            V((pack, LANES), BF16), V((ns, pack, LANES), BF16), V((8, C), F32),
            V((ns, 8, C), F32), V((C, HEAD), F32), V((rows_each, HEAD), F32),
            V((nx, chunks, span, cw), BF16), V((nx, chunks, span, cw), BF16),
            V((nx, chunks, span, cw), BF16), V((nx, chunks, span, cw), BF16),
            DMA((7,)), DMA((nt,)), DMA((nt,)), DMA((nt,)), DMA((nt,)),
            DMA((2, ns, 3)), DMA((ns, 3)), DMA((oth, ns, 3)), DMA((oth, ns, 3)),
            DMA((ns,)), DMA((ns,)), DMA((oth, ns)), DMA((oth, ns)),
            DMA((ns,)), DMA((ns,)), DMA((ns,)), DMA((ns,)), DMA((ns,)), DMA((1,)),
            DMA((nx, chunks)), DMA((nx, chunks)), DMA((nx, chunks)), DMA((nx, chunks)),
        ],
        compiler_params=pltpu.CompilerParams(
            has_side_effects=True, vmem_limit_bytes=60 * 1024 * 1024
        ),
    )(
        tokens[0], norm_gain.astype(F32)[None], w_query, w_forget, w_input, floor_gap[None],
        extra, init_state.reshape(width, HEAD), head_norm_gain.astype(F32)[None], w_output,
    )
    return mixed[None], final.reshape(1, rows_each * HEAD)


def solution(mesh):
    placed = (
        P("grp", ("sp", "tp"), None),
        P(),
        P("sp", None),
        P("sp", None),
        P("sp", None),
        P(),
        P("grp", ("sp", "tp"), None),
        P("grp", None, None, None),
        P(),
        P(None, "sp"),
    )
    return jax.shard_map(
        body,
        mesh=mesh,
        in_specs=placed,
        out_specs=(P("grp", ("sp", "tp"), None), P("grp", ("sp", "tp"))),
        check_vma=False,
    )
```

time: 495 us -> 83.9 us (0.17)
  waiting for transfers between devices: 392 us -> 0 us
  Pallas kernels: 0 us -> 76.8 us
  other arithmetic: 31.6 us -> 1.18 us
  matrix products: 27.9 us -> 0 us
  blocking collectives: 19.4 us -> 0 us
  between operations: 14.3 us -> 0.65 us
    all_gather x5 -> x0, waiting for transfers between devices: 302 us -> none  [the longest x1 79.6 us: body(): forget_sum = add_rows(lax.all_gather(w_forget, 'sp', axis=0, tiled=True))]
    psum x1 -> x0, waiting for transfers between devices: 87.8 us -> none  [broadcast(): return lax.psum(block, axis)]
    pallas_call x0 -> x1, Pallas kernels: none -> 76.8 us  [body(): pl.pallas_call(functools.partial(kernel, (ng, ns, nt, span, D, C, O, chun...]
    dot_general x9 -> x0, matrix products: 27.9 us -> none  [the longest x3 9.64 us: add_rows(): return jnp.dot(normed, piece, preferred_element_type=jnp.float32)]
    select_n x33 -> x0, other arithmetic: 21.8 us -> none  [the longest x32 21.1 us: step(): return jax.tree.map(lambda a, b: jnp.where(reached, a, b), new, before)]
    all_gather x1 -> x0, blocking collectives: 19.4 us -> none  [carried_in(): lax.all_gather(part.astype(kind), axis)]
  transfers between devices with their start and end apart: 6 -> 0, of which waited for: 6 -> 0; matrix products, arithmetic and copies ran while one was open for 11% -> 0% of each run, Pallas kernels for 0% -> 0%
where the time goes in v1:
time: 83.9 us; the launch traced here: 83.5 us
  Pallas kernels  76.8 us (92%)
  local copies, waits for them, and re-layouts  4.85 us (6%)
  other arithmetic  1.18 us (1%)
    pallas_call x1, Pallas kernels, body(): pl.pallas_call(functools.partial(kernel, (ng, ns, nt, span, D, C, O, chun...  76.8 us
    unnamed x8, local copies, waits for them, and re-layouts  2.76 us

profile of v1, /device:TPU:0, one launch (start us, length us, event | category | flops | bytes accessed | tf_op | source)
XLA Modules:
  0.0 83.5 jit_solution(3583659899532228552)
XLA Ops:
  0.6 0.0 copy-start.2
  0.6 0.7 copy-done.2
  1.3 0.0 copy-start.1
  1.3 0.6 broadcast_in_dim.23
  1.9 0.0 copy-start
  1.9 0.1 copy-done.1
  2.0 0.6 broadcast_in_dim.22
  2.6 0.0 copy-done
  2.6 0.1 copy.12
  2.7 0.6 pad.4.extra
  3.3 76.8 %shard_map.113 = (bf16[128,2048]{1,0:T(8,128)(2,1)}, f32[64,64]{1,0:T(8,128)}) custom-call(bf16[128,2048]{1,0:T(8,128)(2,1)} %bitcast.8, f32[1,2048]{1,0:T(1,128)} %bitcast.11, bf16[512,1024]{1,0:T(8,128)(2,1)} %w_query.1, bf16[512,1024]{1,0:T(8,128)(2,1)} %w_forget.1, bf16[512,1024]{1,0:T(8,128)(2,1)} %w_input.1, f32[1,1024]{1,0:T(1,128)} %bitcast.13, ...), custom_call_target="tpu_custom_call" | custom-call | tf_op jit(solution)/shard_map/pallas_call | solution.py:450
  80.2 1.4 %reshape.11 = f32[1,4096]{1,0:T(1,128)} reshape(f32[64,64]{1,0:T(8,128)} %get-tuple-element.5) | data formatting | bytes 32768 | tf_op jit(solution)/shard_map/reshape | solution.py:481
  81.6 1.9 %copy.14 = bf16[1,128,2048]{2,1,0:T(8,128)(2,1)} copy(bf16[1,128,2048]{2,1,0:T(8,128)(2,1)} %bitcast.7) | data formatting | bytes 1048576
Async XLA Ops:
  0.6 0.7 copy-start.2
  1.3 0.7 copy-start.1
  1.9 0.7 copy-start

commit v2 on v1

--- a/solution.py
+++ b/solution.py
@@ -38,7 +38,7 @@
     sizes,
     tokens, norm_gain, w_query, w_forget, w_input, gap, extra, init, head_gain, w_output,
     mixed, final,
-    tok, ext, nrm, wbuf, wout, start, qd, kd, val, etot, bstate, within, gated, carried,
+    tok, ext, nrm, acc, wbuf, wout, start, qd, kd, val, etot, bstate, within, gated, carried,
     st_send, st_recv, dk_send, dk_recv, fin, fin_recv, a_send, a_recv, b_send, b_recv,
     loc, tok_s, tok_r, ext_s, ext_r, z_s, z_r, y_s, y_r, oz_s, oz_r, oy_s, oy_r,
     st_s, st_r, dk_s, dk_r, fin_s, fin_r, as_, ar_, bs_, br_,
@@ -53,6 +53,9 @@
     G = C // LANES
     fold = G % 2 == 0
     weights = (w_query, w_forget, w_input)
+    here = s * nt + t
+    chip, core = lax.div(t, CORES), lax.rem(t, CORES)
+    partner = chip * CORES + 1 - core
     own_cols = pl.ds(pl.multiple_of(t * C, LANES), C)
 
     def remote(src, dst, ssem, rsem, where):
@@ -79,28 +82,55 @@
             pl.ds(pl.multiple_of(who * Ch, 16), Ch), pl.ds(pl.multiple_of(k * OC, LANES), OC)
         ]
 
-    def oz_copy(k, dz):
-        src = w_output.at[pl.ds(pl.multiple_of(t * C + g * Ch, 16), Ch), :]
+    def oz_copy(k, way, src):
+        to = s + 1 if way == 0 else s - 1
+        return remote(src, o_piece(k, g), oz_s.at[way, k], oz_r.at[k], {"sp": to})
+
+    def oy_copy(k, dy, who):
         return remote(
-            src, o_piece(k, g), oz_s.at[dz], oz_r.at[dz], {"sp": lax.rem(s + dz, ns)}
-        )
-
-    def oy_copy(k, dz, dy, who):
-        return remote(
-            o_piece(k, who), o_piece(k, who), oy_s.at[dy - 1, dz], oy_r.at[dy - 1, dz],
+            o_piece(k, who), o_piece(k, who), oy_s.at[dy - 1, k], oy_r.at[dy - 1, k],
             {"grp": lax.rem(g + dy, ng)},
         )
 
-    def tok_copy(dt, slot):
-        return remote(
-            tokens, tok.at[slot], tok_s.at[dt], tok_r.at[dt], {"tp": lax.rem(t + dt, nt)}
-        )
+    def from_chip(dx, side):
+        return lax.rem(chip + nx - dx, nx) * CORES + side
+
+    def tok_copy(src, slot, n, to):
+        return remote(src, tok.at[slot], tok_s.at[n], tok_r.at[slot], {"tp": to})
+
+    def tok_wait(slot):
+        tok_copy(tokens, slot, 0, partner).wait_recv()
 
     def ext_copy(dt, slot):
         return remote(
             extra, ext.at[slot], ext_s.at[dt], ext_r.at[dt], {"tp": lax.rem(t + dt, nt)}
         )
 
+    own_o = w_output.at[pl.ds(pl.multiple_of(t * C + g * Ch, 16), Ch), :]
+    flows = [
+        (way, (lambda d: s - 1 - d) if way == 0 else (lambda d: s + 1 + d),
+         s if way == 0 else ns - 1 - s, (s < ns - 1) if way == 0 else (s > 0))
+        for way in range(2)
+    ]
+
+    barrier = pltpu.get_barrier_semaphore()
+
+    def greet(i, _):
+        other = lax.rem(here + i, ns * nt)
+        pl.semaphore_signal(
+            barrier, inc=1, device_id={"sp": lax.div(other, nt), "tp": lax.rem(other, nt)},
+            device_id_type=pl.DeviceIdType.MESH,
+        )
+        return 0
+
+    for dy in range(1, ng):
+        pl.semaphore_signal(
+            barrier, inc=1, device_id={"grp": lax.rem(g + dy, ng)},
+            device_id_type=pl.DeviceIdType.MESH,
+        )
+    lax.fori_loop(1, ns * nt, greet, 0)
+    pl.semaphore_wait(barrier, ns * nt - 1 + ng - 1)
+
     for a in range(3):
         own = weights[a].at[pl.ds(pl.multiple_of(g * Rh, 16), Rh), own_cols]
 
@@ -112,8 +142,16 @@
         def _():
             z_copy(s, a, 1, own).start()
 
+    for way, _, arrivals, more in flows:
+        @pl.when((arrivals == 0) & more)
+        def _():
+            oz_copy(s, way, own_o).start()
+
+    tok_copy(tokens, t, 0, partner).start()
+    for dx in range(1, nx):
+        to = lax.rem(chip + dx, nx) * CORES + core
+        tok_copy(tokens, t, dx, to).start()
     for dt in range(1, nt):
-        tok_copy(dt, t).start()
         ext_copy(dt, t).start()
     locals_ = [
         pltpu.make_async_copy(tokens, tok.at[t], loc.at[0]),
@@ -149,37 +187,59 @@
             ).astype(BF16)
             return 0
 
-        lax.fori_loop(0, span // rows, step, 0)
+        lax.fori_loop(0, span // rows, step, 0, unroll=True)
 
     locals_[0].wait()
     normalize(t)
 
-    for d in range(max(ns - 1, nt - 1)):
-        if d < ns - 1:
-            for a in range(3):
-                for way in range(2):
-                    k = s - 1 - d if way == 0 else s + 1 + d
-                    valid = k >= 0 if way == 0 else k < ns
-                    more = s < ns - 1 if way == 0 else s > 0
-
-                    @pl.when(valid)
+    tok_wait(partner)
+    normalize(partner)
+
+    for d in range(ns - 1):
+        for a in range(3):
+            for way, shard, arrivals, more in flows:
+                k = shard(d)
+
+                @pl.when(d < arrivals)
+                def _():
+                    z_copy(k, a, way, piece(k, a, g)).wait_recv()
+
+                    @pl.when(more)
                     def _():
-                        z_copy(k, a, way, piece(k, a, g)).wait_recv()
-
-                        @pl.when(more)
-                        def _():
-                            z_copy(k, a, way, piece(k, a, g)).start()
-
-                        for dy in range(1, ng):
-                            y_copy(k, a, dy, g).start()
-            if d == ns - 2:
-                for dz in range(1, ns):
-                    oz_copy(s, dz).start()
-        if d < nt - 1:
-            slot = lax.rem(t + nt - 1 - d, nt)
-            tok_copy(d + 1, slot).wait_recv()
-            normalize(slot)
-            ext_copy(d + 1, slot).wait_recv()
+                        z_copy(k, a, way, piece(k, a, g)).start()
+
+                    for dy in range(1, ng):
+                        y_copy(k, a, dy, g).start()
+        for way, _, arrivals, more in flows:
+            @pl.when((arrivals == d + 1) & more)
+            def _():
+                oz_copy(s, way, own_o).start()
+        if d == min(1, ns - 2):
+            for dx in range(1, nx):
+                slot = from_chip(dx, core)
+                tok_wait(slot)
+                tok_copy(tok.at[slot], slot, nx - 1 + dx, partner).start()
+                normalize(slot)
+    for dx in range(1, nx):
+        slot = from_chip(dx, 1 - core)
+        tok_wait(slot)
+        normalize(slot)
+
+    def o_step(e, onward):
+        for way, shard, arrivals, more in flows:
+            k = shard(e)
+            when = (e < arrivals) & (more if onward else jnp.logical_not(more))
+
+            @pl.when(when)
+            def _():
+                oz_copy(k, way, own_o).wait_recv()
+                if onward:
+                    oz_copy(k, way, o_piece(k, g)).start()
+                for dy in range(1, ng):
+                    oy_copy(k, dy, g).start()
+
+    for e in range(ns - 1):
+        o_step(e, True)
 
     for copy in locals_[1:]:
         copy.wait()
@@ -192,13 +252,34 @@
         for dy in range(1, ng):
             y_copy(k, a, dy, lax.rem(g + ng - dy, ng)).wait_recv()
 
-    for dz in range(1, ns):
-        for a in range(3):
-            y_wait(lax.rem(s + dz, ns), a)
+    def add(k, first):
+        deep = pl.ds(pl.multiple_of(k * R, LANES), R)
+
+        def step(m, _):
+            rows = pl.ds(pl.multiple_of(m * span, span), span)
+            more = jnp.dot(nrm[rows, deep], wbuf[deep, :], preferred_element_type=F32)
+            acc[rows, :] = more if first else acc[rows, :] + more
+            return 0
+
+        lax.fori_loop(0, nt, step, 0)
+
+    add(s, True)
+    for d in range(ns - 1):
+        for _, shard, arrivals, _ in flows:
+            k = shard(d)
+
+            @pl.when(d < arrivals)
+            def _():
+                for a in range(3):
+                    y_wait(k, a)
+                add(k, False)
+
+    for dt in range(1, nt):
+        ext_copy(dt, lax.rem(t + nt - dt, nt)).wait_recv()
 
     floor = gap[:, own_cols]
     heads = (
-        iota((LANES, C), 0) == iota((LANES, C), 1) // HEAD + t * (C // HEAD)
+        iota((ext.shape[1], C), 0) == iota((ext.shape[1], C), 1) // HEAD + t * (C // HEAD)
     ).astype(F32)
     tri = (
         (iota((span, span), 0) >= iota((span, span), 1)) & same_group(span, span, BLOCK)
@@ -208,17 +289,11 @@
 
     def project(m, _):
         rows = pl.ds(pl.multiple_of(m * span, span), span)
-        x = nrm[rows, :]
-        raw = [
-            jnp.dot(x, wbuf[:, a * C:(a + 1) * C], preferred_element_type=F32).astype(BF16)
-            for a in range(3)
-        ]
+        raw = [acc[rows, a * C:(a + 1) * C].astype(BF16) for a in range(3)]
         query = raw[0].astype(F32)
         query = query / (1.0 + jnp.exp(-query))
         key = floor / (1.0 + jnp.exp(raw[1].astype(F32)))
-        log_keep = jnp.log1p(-key) + jnp.dot(
-            ext[m], heads, precision=HIGHEST, preferred_element_type=F32
-        )
+        log_keep = jnp.log1p(-key) + contract(ext[m], heads, 0, 0, HIGHEST)
         cumul = jnp.dot(tri, log_keep, precision=HIGHEST, preferred_element_type=F32)
         qd[rows, :] = (query * jnp.exp(cumul)).astype(BF16)
         kd[rows, :] = (key * jnp.exp(-cumul)).astype(BF16)
@@ -236,7 +311,10 @@
             dk_send[...] = dk_send[...] * decay
         return 0
 
-    lax.fori_loop(0, nt, project, 0)
+    half = nt // 2
+    lax.fori_loop(0, half, project, 0)
+    o_step(0, False)
+    lax.fori_loop(half, nt, project, 0)
 
     tiles = [slice(i * LANES, (i + 1) * LANES) for i in range(G)]
     if fold:
@@ -261,11 +339,8 @@
             st_copy(dz, s).start()
             dk_copy(dz, s).start()
 
-    for dz in range(1, ns):
-        k = lax.rem(s + ns - dz, ns)
-        oz_copy(k, dz).wait_recv()
-        for dy in range(1, ng):
-            oy_copy(k, dz, dy, g).start()
+    for e in range(1, ns - 1):
+        o_step(e, False)
 
     copies = C // HEAD
     wide = copies * BLOCK
@@ -315,8 +390,6 @@
     lax.fori_loop(0, nblk, read, 0)
 
     rows_each = final.shape[0]
-    here = s * nt + t
-
     def fin_copy(i, where):
         return remote(
             fin.at[pl.ds(i * rows_each, rows_each), :], fin_recv, fin_s.at[i], fin_r.at[0],
@@ -340,11 +413,9 @@
                 final[...] = fin[i * rows_each:(i + 1) * rows_each, :]
 
     for dz in range(1, ns):
-        k = lax.rem(s + ns - dz, ns)
         for dy in range(1, ng):
-            oy_copy(k, dz, dy, lax.rem(g + ng - dy, ng)).wait_recv()
-
-    chip, core = lax.div(t, CORES), lax.rem(t, CORES)
+            oy_copy(lax.rem(s + dz, ns), dy, lax.rem(g + ng - dy, ng)).wait_recv()
+
     cw = O // chunks
 
     def product(dx, side, j):
@@ -355,7 +426,7 @@
     def a_copy(dx, j):
         return remote(
             a_send.at[dx, j], a_recv.at[dx, j], as_.at[dx, j], ar_.at[dx, j],
-            {"tp": chip * CORES + 1 - core},
+            {"tp": partner},
         )
 
     def b_copy(dx, j):
@@ -402,13 +473,20 @@
         for dz in range(1, ns):
             for dy in range(1, ng):
                 y_copy(lax.rem(s + dz, ns), a, dy, g).wait_send()
+    for way, _, arrivals, more in flows:
+        for d in range(ns):
+            k = s - d if way == 0 else s + d
+
+            @pl.when((d <= arrivals) & more)
+            def _():
+                oz_copy(k, way, own_o).wait_send()
+    for n in range(2 * nx - 1):
+        tok_copy(tokens, t, n, partner).wait_send()
     for dt in range(1, nt):
-        tok_copy(dt, t).wait_send()
         ext_copy(dt, t).wait_send()
     for dz in range(1, ns):
-        oz_copy(s, dz).wait_send()
         for dy in range(1, ng):
-            oy_copy(lax.rem(s + ns - dz, ns), dz, dy, g).wait_send()
+            oy_copy(lax.rem(s + dz, ns), dy, g).wait_send()
 
         @pl.when(s + dz < ns)
         def _():
@@ -445,7 +523,7 @@
     cw = O // chunks
     V, DMA = pltpu.VMEM, pltpu.SemaphoreType.DMA
     any_, vmem = pl.BlockSpec(memory_space=pl.ANY), pl.BlockSpec(memory_space=pltpu.VMEM)
-    extra = jnp.pad(extra_decay[0], ((0, 0), (0, LANES - heads)))
+    extra = extra_decay[0].T
     oth = max(ng - 1, 1)
     mixed, final = pl.pallas_call(
         functools.partial(kernel, (ng, ns, nt, span, D, C, O, chunks)),
@@ -456,7 +534,7 @@
         in_specs=[any_, vmem, any_, any_, any_, vmem, any_, any_, vmem, any_],
         out_specs=(vmem, vmem),
         scratch_shapes=[
-            V((nt, span, D), BF16), V((nt, span, LANES), F32), V((T, D), BF16),
+            V((nt, span, D), BF16), V((nt, heads, span), F32), V((T, D), BF16), V((T, 3 * C), F32),
             V((D, 3 * C), BF16), V((C, O), BF16), V((C, HEAD), F32),
             V((T, C), BF16), V((T, C), BF16), V((T, C), BF16),
             V((nblk, 8, C), F32), V((nblk, C, C), F32), V((T, C), F32), V((T, C), BF16),
@@ -465,14 +543,14 @@
             V((ns, 8, C), F32), V((C, HEAD), F32), V((rows_each, HEAD), F32),
             V((nx, chunks, span, cw), BF16), V((nx, chunks, span, cw), BF16),
             V((nx, chunks, span, cw), BF16), V((nx, chunks, span, cw), BF16),
-            DMA((7,)), DMA((nt,)), DMA((nt,)), DMA((nt,)), DMA((nt,)),
+            DMA((7,)), DMA((2 * nx,)), DMA((nt,)), DMA((nt,)), DMA((nt,)),
             DMA((2, ns, 3)), DMA((ns, 3)), DMA((oth, ns, 3)), DMA((oth, ns, 3)),
-            DMA((ns,)), DMA((ns,)), DMA((oth, ns)), DMA((oth, ns)),
+            DMA((2, ns)), DMA((ns,)), DMA((oth, ns)), DMA((oth, ns)),
             DMA((ns,)), DMA((ns,)), DMA((ns,)), DMA((ns,)), DMA((ns,)), DMA((1,)),
             DMA((nx, chunks)), DMA((nx, chunks)), DMA((nx, chunks)), DMA((nx, chunks)),
         ],
         compiler_params=pltpu.CompilerParams(
-            has_side_effects=True, vmem_limit_bytes=60 * 1024 * 1024
+            collective_id=0, has_side_effects=True, vmem_limit_bytes=60 * 1024 * 1024
         ),
     )(
         tokens[0], norm_gain.astype(F32)[None], w_query, w_forget, w_input, floor_gap[None],

time: 83.9 us -> 74.6 us (0.89)
  Pallas kernels: 76.8 us -> 68.3 us
    pallas_call x1, Pallas kernels: 76.8 us -> 68.3 us  [body(): pl.pallas_call(functools.partial(kernel, (ng, ns, nt, span, D, C, O, chun...]
    unnamed x8 -> x5, local copies, waits for them, and re-layouts: 2.76 us -> 2.65 us
where the time goes in v2:
time: 74.6 us; the launch traced here: 74.2 us
  Pallas kernels  68.3 us (92%)
  local copies, waits for them, and re-layouts  4.1 us (5%)
  other arithmetic  1.19 us (2%)
    pallas_call x1, Pallas kernels, body(): pl.pallas_call(functools.partial(kernel, (ng, ns, nt, span, D, C, O, chun...  68.3 us
    unnamed x5, local copies, waits for them, and re-layouts  2.65 us

profile of v2, /device:TPU:0, one launch (start us, length us, event | category | flops | bytes accessed | tf_op | source)
XLA Modules:
  0.0 74.2 jit_solution(8296338551676185735)
XLA Ops:
  0.6 0.0 copy-start.1
  0.6 0.7 copy-done.1
  1.3 0.0 copy-start
  1.3 0.6 broadcast_in_dim.23
  1.9 0.1 copy-done
  2.0 0.6 broadcast_in_dim.22
  2.6 68.3 %shard_map.113 = (bf16[128,2048]{1,0:T(8,128)(2,1)}, f32[64,64]{1,0:T(8,128)}) custom-call(bf16[128,2048]{1,0:T(8,128)(2,1)} %bitcast.9, f32[1,2048]{1,0:T(1,128)} %bitcast.12, bf16[512,1024]{1,0:T(8,128)(2,1)} %w_query.1, bf16[512,1024]{1,0:T(8,128)(2,1)} %w_forget.1, bf16[512,1024]{1,0:T(8,128)(2,1)} %w_input.1, f32[1,1024]{1,0:T(1,128)} %bitcast.15, ...), custom_call_target="tpu_custom_call" | custom-call | tf_op jit(solution)/shard_map/pallas_call | solution.py:528
  70.9 1.4 %reshape.11 = f32[1,4096]{1,0:T(1,128)} reshape(f32[64,64]{1,0:T(8,128)} %get-tuple-element.5) | data formatting | bytes 32768 | tf_op jit(solution)/shard_map/reshape | solution.py:559
  72.3 1.9 %copy.13 = bf16[1,128,2048]{2,1,0:T(8,128)(2,1)} copy(bf16[1,128,2048]{2,1,0:T(8,128)(2,1)} %bitcast.11) | data formatting | bytes 1048576
Async XLA Ops:
  0.6 0.7 copy-start.1
  1.3 0.7 copy-start
